TPU v7x, 32 devices: a whole 2x2x4 slice. The times are simulated.
32 devices in a mesh: sp: 8 (over z, x), tp: 4 (over y, core).
Axes of the slice: x: 2, y: 2, z: 4, core: 2. Of those that a mesh axis runs over, the one named last changes fastest.
Arguments:
- tokens_in: bfloat16 [6144, 2048], P(('sp', 'tp')), may hold values from -300 to 300
- norm_gain: float32 [2048], replicated, may hold values from 0.1 to 1.9
- query_weight: bfloat16 [2048, 1024], P('sp', 'tp'), may hold values from -64 to 64
- key_weight: bfloat16 [2048, 512], P('sp', 'tp'), may hold values from -1 to 1
- value_weight: bfloat16 [2048, 512], P('sp', 'tp'), may hold values from -0.125 to 0.125
- pool_weight: bfloat16 [2048, 1024], P('sp', 'tp'), may hold values from -0.125 to 0.125
- sink_logit: float32 [16], P('tp'), may hold values from 1 to 5
- pool_gain: float32 [1024], P('tp'), may hold values from 0.1 to 1.9
- attention_out_weight: bfloat16 [1024, 2048], P('tp', 'sp'), may hold values from -0.125 to 0.125
- pool_out_weight: bfloat16 [1024, 2048], P('tp', 'sp'), may hold values from -0.1875 to 0.1875
Outputs:
- mixed_out: bfloat16 [6144, 2048], P(('sp', 'tp'))
All inputs are finite; a program needn't handle non-finite values.
Results may differ from a plain program's by a relative error of at most 0.014.
Values may be sent and summed in bfloat16 or wider, within the bound.
A program may use at most 64 MiB of HBM per device.

v0:
```python
import jax
import jax.numpy as jnp
from jax import lax
from jax.sharding import PartitionSpec as P

HEAD_DIM = 64
POOL_CH = 256
POOL_GROUPS = 4
WINDOW = 128


EPS = 1e-06
SHORT_REACHES = (8, 32)


def passed_along(block, axis, distance):
    devices = range(lax.axis_size(axis))
    route = [(i - distance, i) for i in devices if i - distance in devices]
    return lax.ppermute(block, axis, route)


def local(
    tokens_in,
    norm_gain,
    query_weight,
    key_weight,
    value_weight,
    pool_weight,
    sink_logit,
    pool_gain,
    attention_out_weight,
    pool_out_weight,
):
    widened = tokens_in.astype(jnp.float32)
    inverse = lax.rsqrt(jnp.mean(widened * widened, axis=1, keepdims=True) + EPS)
    normed = (widened * inverse * norm_gain).astype(jnp.bfloat16)
    all_rows = lax.all_gather(normed, "tp", axis=0, tiled=True)
    pieces = (
        lax.all_gather(query_weight, "sp", axis=0, tiled=True),
        lax.all_gather(key_weight, "sp", axis=0, tiled=True),
        lax.all_gather(value_weight, "sp", axis=0, tiled=True),
        lax.all_gather(pool_weight, "sp", axis=0, tiled=True),
    )
    projected = tuple(
        (
            jnp.dot(all_rows, weight_piece, preferred_element_type=jnp.float32)
            for weight_piece in pieces
        )
    )
    query_rows, key_rows, value_rows, pool_rows = [
        projection.astype(jnp.bfloat16) for projection in projected
    ]
    seq_len = query_rows.shape[0]
    offset = lax.axis_index("sp") * seq_len
    halo_keys, halo_values, halo_pool = passed_along(
        (
            key_rows[seq_len - WINDOW :],
            value_rows[seq_len - WINDOW :],
            pool_rows[seq_len - WINDOW :],
        ),
        "sp",
        1,
    )
    kv_local = key_rows.shape[1] // HEAD_DIM
    heads_local = query_rows.shape[1] // HEAD_DIM
    group = heads_local // kv_local
    blocks = seq_len // WINDOW
    key_ext = jnp.concatenate([halo_keys, key_rows], axis=0).reshape(
        blocks + 1, WINDOW, kv_local, HEAD_DIM
    )
    value_ext = jnp.concatenate([halo_values, value_rows], axis=0).reshape(
        blocks + 1, WINDOW, kv_local, HEAD_DIM
    )
    key_pairs = jnp.concatenate([key_ext[:-1], key_ext[1:]], axis=1)
    value_pairs = jnp.concatenate([value_ext[:-1], value_ext[1:]], axis=1)
    query_blocks = query_rows.reshape(blocks, WINDOW, kv_local, group, HEAD_DIM)
    scores = jnp.einsum(
        "nqhgd,nkhd->nhgqk", query_blocks, key_pairs, preferred_element_type=jnp.float32
    ) * HEAD_DIM ** (-0.5)
    shape_mask = (blocks, WINDOW, 2 * WINDOW)
    q_index = lax.broadcasted_iota(jnp.int32, shape_mask, 1)
    k_index = lax.broadcasted_iota(jnp.int32, shape_mask, 2)
    block_index = lax.broadcasted_iota(jnp.int32, shape_mask, 0)
    distance = q_index + WINDOW - k_index
    key_position = offset + block_index * WINDOW + k_index - WINDOW
    allowed = (distance >= 0) & (distance < WINDOW) & (key_position >= 0)
    scores = jnp.where(allowed[:, None, None], scores, -jnp.inf)
    sinks = sink_logit.reshape(1, kv_local, group, 1, 1)
    peak = jnp.maximum(jnp.max(scores, axis=-1, keepdims=True), sinks)
    expo = jnp.exp(scores - peak)
    denom = jnp.sum(expo, axis=-1, keepdims=True) + jnp.exp(sinks - peak)
    probs = (expo / denom).astype(jnp.bfloat16)
    attended = jnp.einsum(
        "nhgqk,nkhd->nqhgd", probs, value_pairs, preferred_element_type=jnp.float32
    )
    attended = attended.astype(jnp.bfloat16).reshape(seq_len, heads_local * HEAD_DIM)
    pool_values = pool_rows.astype(jnp.float32)
    channels = pool_rows.shape[1]
    pool_ext = jnp.concatenate([halo_pool.astype(jnp.float32), pool_values], axis=0)
    running = jnp.concatenate(
        [jnp.zeros((1, channels), jnp.float32), jnp.cumsum(pool_ext, axis=0)], axis=0
    )
    group_id = lax.axis_index("tp") * channels // POOL_CH
    reach = jnp.where(
        group_id == 0, SHORT_REACHES[0], jnp.where(group_id == 1, SHORT_REACHES[1], WINDOW)
    ).astype(jnp.int32)
    upper = running[WINDOW + 1 :]
    lower = lax.dynamic_slice_in_dim(running, WINDOW + 1 - reach, seq_len, 0)
    position = offset + lax.broadcasted_iota(jnp.int32, (seq_len,), 0)
    counted = jnp.minimum(position + 1, reach).astype(jnp.float32)[:, None]
    windowed = (upper - lower) / counted
    own_sums = upper - running[WINDOW]
    device_total = own_sums[seq_len - 1]
    totals = lax.all_gather(device_total[None, :], "sp", axis=0, tiled=True)
    earlier_rows = lax.broadcasted_iota(jnp.int32, (totals.shape[0], 1), 0) < lax.axis_index("sp")
    before = jnp.sum(jnp.where(earlier_rows, totals, 0.0), axis=0)
    cumulative = (before[None, :] + own_sums) / (position + 1).astype(jnp.float32)[:, None]
    pooled = jnp.where(group_id == POOL_GROUPS - 1, cumulative, windowed)
    pool_mixed = ((pooled - pool_values) * pool_gain).astype(jnp.bfloat16)
    out_attend, out_pool = (
        lax.all_gather(attention_out_weight, "sp", axis=1, tiled=True),
        lax.all_gather(pool_out_weight, "sp", axis=1, tiled=True),
    )
    return lax.psum_scatter(
        (
            jnp.dot(attended, out_attend, preferred_element_type=jnp.float32)
            + jnp.dot(pool_mixed, out_pool, preferred_element_type=jnp.float32)
        ).astype(jnp.bfloat16),
        "tp",
        scatter_dimension=0,
        tiled=True,
    )


def solution(mesh):
    in_specs = (
        P(("sp", "tp"), None),
        P(),
        P("sp", "tp"),
        P("sp", "tp"),
        P("sp", "tp"),
        P("sp", "tp"),
        P("tp"),
        P("tp"),
        P("tp", "sp"),
        P("tp", "sp"),
    )
    out_specs = P(("sp", "tp"), None)
    return jax.shard_map(local, mesh=mesh, in_specs=in_specs, out_specs=out_specs, check_vma=False)
```

profile of v0, /device:TPU:0, one launch (start us, length us, event | category | flops | bytes accessed | tf_op | source)
XLA Modules:
  0.0 258.5 jit_solution(11040863534690571767)
XLA Ops:
  6.5 1.4 fusion.2
  8.0 2.3 fusion.4
  10.3 0.7 all-gather.13.cloned.1.call-update
  11.0 0.7 all-gather.9.cloned.1.call-update
  11.8 0.5 all-gather.11.cloned.1.call-update
  12.4 0.5 all-gather.15.cloned.1.call-update
  13.1 33.1 %all_gather.26 = bf16[2048,128]{1,0:T(8,128)(2,1)S(1)} all-gather(bf16[256,128]{1,0:T(8,128)(2,1)S(1)} %copy-done.2), channel_id=1, replica_groups=mesh['sp'=8,'tp'=4] {'sp'}, dimensions={0}, use_global_device_ids=true | all-gather | bytes 589824 | tf_op jit(solution)/shard_map/all_gather | solution.py:40
  46.3 32.4 %all_gather.25 = bf16[2048,128]{1,0:T(8,128)(2,1)S(1)} all-gather(bf16[256,128]{1,0:T(8,128)(2,1)S(1)} %copy-done.3), channel_id=1, replica_groups=mesh['sp'=8,'tp'=4] {'sp'}, dimensions={0}, use_global_device_ids=true | all-gather | bytes 589824 | tf_op jit(solution)/shard_map/all_gather | solution.py:41
  79.0 2.9 %convolution_convert_fusion.2 = bf16[768,128]{1,0:T(8,128)(2,1)S(1)} fusion(bf16[768,2048]{1,0:T(8,128)(2,1)} %all-gather.7.cloned.1.call-done, bf16[2048,128]{1,0:T(8,128)(2,1)S(1)} %all_gather.26), kind=kOutput, calls=%fused_computation.16 | convolution fusion | flops 402751488 | bytes 3866624 | tf_op jit(solution)/shard_map/dot_general | solution.py:46
  81.9 0.6 slice.59
  82.5 3.9 %collective-permute-start.1 = (bf16[128,128]{1,0:T(8,128)(2,1)}, bf16[128,128]{1,0:T(8,128)(2,1)}, u32[]{:S(2)}, u32[]{:S(2)}) collective-permute-start(bf16[128,128]{1,0:T(8,128)(2,1)} %slice.59), channel_id=1, source_target_pairs={{0,4},{4,8},{8,12},{12,16},{16,20},{20,24},{24,28},{1,5},{5,9},{9,... | collective-permute-start | bytes 98312 | tf_op jit(solution)/shard_map/ppermute | solution.py:19
  86.4 0.6 all-gather.13.cloned.1.call-done
  87.0 3.2 %fusion.44 = (f32[768,256]{1,0:T(8,128)S(1)}, bf16[768,256]{1,0:T(8,128)(2,1)S(1)}) fusion(bf16[768,2048]{1,0:T(8,128)(2,1)} %all-gather.7.cloned.1.call-done, bf16[2048,256]{1,0:T(8,128)(2,1)} %all-gather.13.cloned.1.call-done), kind=kOutput, calls=%fused_computation.74 | convolution fusion | flops 805699584 | bytes 5373952 | tf_op jit(solution)/shard_map/dot_general | solution.py:46
  90.2 0.6 slice.60
  90.8 2.0 collective-permute-start.2
  92.8 35.4 %all-gather.9.cloned.1.call-done = bf16[2048,256]{1,0:T(8,128)(2,1)} async-done(((bf16[256,256]{1,0:T(8,128)(2,1)}), bf16[2048,256]{1,0:T(8,128)(2,1)}) %all-gather.9.cloned.1.call-update) | async-done | bytes 1048592 | tf_op jit(solution)/shard_map/all_gather | solution.py:39
  128.2 3.3 %convolution_convert_fusion.1 = bf16[768,256]{1,0:T(8,128)(2,1)S(1)} fusion(bf16[768,2048]{1,0:T(8,128)(2,1)} %all-gather.7.cloned.1.call-done, bf16[2048,256]{1,0:T(8,128)(2,1)} %all-gather.9.cloned.1.call-done), kind=kOutput, calls=%fused_computation.13 | convolution fusion | flops 805502976 | bytes 4587520 | tf_op jit(solution)/shard_map/dot_general | solution.py:46
  131.5 1.0 convolution_convert_fusion.3
  132.8 2.5 collective-permute-start
  135.3 1.0 copy.40
  136.3 1.0 copy.36
  137.6 0.8 pad_maximum_fusion.1
  139.6 0.7 fusion.1
  140.4 0.7 fusion
  141.2 0.9 fusion.7
  142.4 25.8 %all-gather.11.cloned.1.call-done = bf16[256,2048]{1,0:T(8,128)(2,1)} async-done(((bf16[256,256]{1,0:T(8,128)(2,1)}), bf16[256,2048]{1,0:T(8,128)(2,1)}) %all-gather.11.cloned.1.call-update) | async-done | bytes 1048592 | tf_op jit(solution)/shard_map/all_gather | solution.py:121
  168.2 4.9 %fusion.23 = f32[768,2048]{1,0:T(8,128)} fusion(bf16[256,2048]{1,0:T(8,128)(2,1)} %all-gather.11.cloned.1.call-done, bf16[32,8,6,128]{3,2,1,0:T(8,128)(2,1)S(1)} %bitcast.64), kind=kOutput, calls=%fused_computation.38 | convolution fusion | flops 805306368 | bytes 7733248 | tf_op jit(solution)/shard_map/dot_general | solution.py:126
  173.2 0.7 fusion.8
  174.4 18.4 %all-gather = f32[8,1,256]{2,1,0:T(1,128)S(1)} all-gather(f32[1,1,256]{2,1,0:T(1,128)S(1)} %slice_bitcast_fusion.1), channel_id=1, replica_groups=mesh['sp'=8,'tp'=4] {'sp'}, dimensions={0}, use_global_device_ids=true | all-gather | bytes 9216 | tf_op jit(solution)/shard_map/all_gather | solution.py:114
  192.9 15.6 %all-gather.15.cloned.1.call-done = bf16[256,2048]{1,0:T(8,128)(2,1)} async-done(((bf16[256,256]{1,0:T(8,128)(2,1)}), bf16[256,2048]{1,0:T(8,128)(2,1)}) %all-gather.15.cloned.1.call-update) | async-done | bytes 1048592 | tf_op jit(solution)/shard_map/all_gather | solution.py:122
  208.5 6.1 %add_convert_fusion = bf16[768,2048]{1,0:T(8,128)(2,1)} fusion(f32[768,2048]{1,0:T(8,128)} %fusion.23, bf16[256,2048]{1,0:T(8,128)(2,1)} %all-gather.15.cloned.1.call-done, s32[]{:T(128)S(6)} %select_n.38, f32[896,256]{1,0:T(8,128)S(1)} %bitcast.62, f32[768,256]{1,0:T(8,128)S(1)} %slice_subtract_fusion, f32[256]{0:T(256)S(1)} %copy-done.4, ...), kind=kOutput, calls=%fused_computation | convolution fusion | flops 810221568 | bytes 13379589 | tf_op jit(solution)/shard_map/dot_general | solution.py:127
  214.6 37.0 %reduce-scatter.2.cloned.1.call-done = bf16[192,2048]{1,0:T(8,128)(2,1)} async-done(((bf16[768,2048]{1,0:T(8,128)(2,1)}), bf16[192,2048]{1,0:T(8,128)(2,1)}) %reduce-scatter.2.cloned.1.call-update) | async-done | bytes 786448 | tf_op jit(solution)/shard_map/reduce_scatter | solution.py:124
  (55 shorter events, 3.5 us)
Async XLA Ops:
  6.5 6.5 %copy-start.6 = (f32[4]{0:T(128)S(1)}, f32[4]{0:T(128)}, u32[]{:S(2)}) copy-start(f32[4]{0:T(128)} %param.16) | copy-start | bytes 52
  6.5 6.6 %copy-start.2 = (bf16[256,128]{1,0:T(8,128)(2,1)S(1)}, bf16[256,128]{1,0:T(8,128)(2,1)}, u32[]{:S(2)}) copy-start(bf16[256,128]{1,0:T(8,128)(2,1)} %param.13) | copy-start | bytes 196612
  6.5 39.7 %copy-start.3 = (bf16[256,128]{1,0:T(8,128)(2,1)S(1)}, bf16[256,128]{1,0:T(8,128)(2,1)}, u32[]{:S(2)}) copy-start(bf16[256,128]{1,0:T(8,128)(2,1)} %param.14) | copy-start | bytes 196612
  6.5 72.5 %all-gather.7.cloned.1.call-start = ((), (), s32[]{:S(2)}) async-start(), calls=%async_computation.1 | async-start | bytes 3932160 | tf_op jit(solution)/shard_map/all_gather | solution.py:37
  10.2 76.7 %all-gather.13.cloned.1.call-start = ((), (), s32[]{:S(2)}) async-start(), calls=%async_computation.4 | async-start | bytes 1179648 | tf_op jit(solution)/shard_map/all_gather | solution.py:42
  11.0 117.2 %all-gather.9.cloned.1.call-start = ((), (), s32[]{:S(2)}) async-start(), calls=%async_computation.2 | async-start | bytes 1179648 | tf_op jit(solution)/shard_map/all_gather | solution.py:39
  11.7 156.5 %all-gather.11.cloned.1.call-start = ((), (), s32[]{:S(2)}) async-start(), calls=%async_computation.3 | async-start | bytes 1179648 | tf_op jit(solution)/shard_map/all_gather | solution.py:121
  12.3 196.2 %all-gather.15.cloned.1.call-start = ((), (), s32[]{:S(2)}) async-start(), calls=%async_computation.5 | async-start | bytes 1179648 | tf_op jit(solution)/shard_map/all_gather | solution.py:122
  12.9 238.8 %reduce-scatter.2.cloned.1.call-start = ((), (), s32[]{:S(2)}) async-start(), calls=%async_computation.6 | async-start | bytes 3932160 | tf_op jit(solution)/shard_map/reduce_scatter | solution.py:124
  82.5 55.1 %collective-permute-start.1 = (bf16[128,128]{1,0:T(8,128)(2,1)}, bf16[128,128]{1,0:T(8,128)(2,1)}, u32[]{:S(2)}, u32[]{:S(2)}) collective-permute-start(bf16[128,128]{1,0:T(8,128)(2,1)} %slice.59), channel_id=1, source_target_pairs={{0,4},{4,8},{8,12},{12,16},{16,20},{20,24},{24,28},{1,5},{5,9},{9,... | collective-permute-start | bytes 98312 | tf_op jit(solution)/shard_map/ppermute | solution.py:19
  90.8 82.3 %collective-permute-start.2 = (bf16[128,256]{1,0:T(8,128)(2,1)}, bf16[128,256]{1,0:T(8,128)(2,1)S(1)}, u32[]{:S(2)}, u32[]{:S(2)}) collective-permute-start(bf16[128,256]{1,0:T(8,128)(2,1)} %slice.60), channel_id=1, source_target_pairs={{0,4},{4,8},{8,12},{12,16},{16,20},{20,24},{24,28},{1,5},{5,9},{9,... | collective-permute-start | bytes 196616 | tf_op jit(solution)/shard_map/ppermute | solution.py:19
  128.2 3.3 %copy-start.5 = (bf16[768,2048]{1,0:T(8,128)(2,1)S(1)}, bf16[768,2048]{1,0:T(8,128)(2,1)}, u32[]{:S(2)}) copy-start(bf16[768,2048]{1,0:T(8,128)(2,1)} %all-gather.7.cloned.1.call-done) | copy-start | bytes 9437188
  132.8 6.1 %collective-permute-start = (bf16[128,128]{1,0:T(8,128)(2,1)S(1)}, bf16[128,128]{1,0:T(8,128)(2,1)S(1)}, u32[]{:S(2)}, u32[]{:S(2)}) collective-permute-start(bf16[128,128]{1,0:T(8,128)(2,1)S(1)} %slice.58), channel_id=1, source_target_pairs={{0,4},{4,8},{8,12},{12,16},{16,20},{20,24},{24,28},{1,5},{5,9},{9,... | collective-permute-start | bytes 98312 | tf_op jit(solution)/shard_map/ppermute | solution.py:19
  137.6 2.0 copy-start.1
  139.6 1.6 copy-start
  173.9 34.7 %copy-start.4 = (f32[256]{0:T(256)S(1)}, f32[256]{0:T(256)}, u32[]{:S(2)}) copy-start(f32[256]{0:T(256)} %param.17) | copy-start | bytes 3076
Sparse Core Ops, SparseCore 0:
  10.4 31.2 all-gather.6
  43.8 43.1 all-gather.12
  89.1 38.9 all-gather.8
  130.1 38.0 all-gather.10
  170.1 38.4 all-gather.14
  214.7 36.8 reduce-scatter.1
where the time goes:
time: 259 us
  waiting for transfers between devices  117 us (45%)
  blocking collectives  84 us (32%)
  matrix products  22.9 us (9%)
  between operations  13.8 us (5%)
  starting transfers between devices  8.61 us (3%)
  other arithmetic  6.68 us (3%)
  local copies, waits for them, and re-layouts  5.6 us (2%)
    reduce_scatter x1, waiting for transfers between devices, local(): lax.psum_scatter((jnp.dot(attended, out_attend, preferred_element_type=jn...  37 us
    all_gather x1, waiting for transfers between devices, local(): lax.all_gather(query_weight, 'sp', axis=0, tiled=True)  35.4 us
    all_gather x1, blocking collectives, local(): lax.all_gather(key_weight, 'sp', axis=0, tiled=True)  33.1 us
    all_gather x1, blocking collectives, local(): lax.all_gather(value_weight, 'sp', axis=0, tiled=True)  32.4 us
    all_gather x1, waiting for transfers between devices, local(): lax.all_gather(attention_out_weight, 'sp', axis=1, tiled=True)  25.8 us
    all_gather x1, blocking collectives, local(): totals = lax.all_gather(device_total[None, :], 'sp', axis=0, tiled=True)  18.4 us
    all_gather x1, waiting for transfers between devices, local(): lax.all_gather(pool_out_weight, 'sp', axis=1, tiled=True)  15.6 us
    dot_general x4, matrix products, local(): jnp.dot(all_rows, weight_piece, preferred_element_type=jnp.float32)  10.3 us
  transfers between devices with their start and end apart: 9, of which 5 were waited for; matrix products, arithmetic and copies ran while one was open for 10% of the time, Pallas kernels for 0%

commit v1 on v0

v1 whole, which is shorter than its diff:
```python
import functools
import math

import jax
import jax.numpy as jnp
from jax import lax
from jax.experimental import pallas as pl
from jax.experimental.pallas import tpu as pltpu
from jax.sharding import PartitionSpec as P

HEAD_DIM = 64
POOL_CH = 256
POOL_GROUPS = 4
WINDOW = 128
EPS = 1e-06
SHORT_REACHES = (8, 32)
CORES = 2
SIDE_SHARE = 6
MESH = pl.DeviceIdType.MESH
F32 = jnp.float32
BF16 = jnp.bfloat16


def row_tile(rows, most):
    tile = most
    while rows % tile:
        tile -= 16
    return tile


def kernel(n_sp, n_tp, cols, n_in, n_out, widths, *refs):
    tok, gain, sink, pgain = refs[:4]
    win_refs = refs[4 : 4 + n_in]
    wout_refs = refs[4 + n_in : 4 + n_in + n_out]
    (
        out, xs, wi, wo, acc, ext, mix, tot, carry, dsend, drecv, ysend, yrecv, own,
        local_sem, send_sem, sem_in, sem_in_side, sem_out, sem_out_side,
        sem_tok, sem_halo, sem_tot, sem_core, sem_y,
    ) = refs[4 + n_in + n_out :]
    qw, kw, vw, pw = widths
    levels = n_sp // cols
    chips = n_tp // CORES
    rows, seq = tok.shape[0], xs.shape[1]
    piece = xs.shape[2]
    blocks = seq // WINDOW
    me, t = lax.axis_index("sp"), lax.axis_index("tp")
    z, x = me // cols, me % cols
    y, c = t // CORES, t % CORES
    partner = y * CORES + (1 - c)

    locals_ = []
    at = 0
    for i, ref in enumerate(win_refs):
        w = ref.shape[1]
        locals_.append(pltpu.make_async_copy(ref, wi.at[me, :, pl.ds(at, w)], local_sem.at[i]))
        at += w
    at = 0
    for i, ref in enumerate(wout_refs):
        k = ref.shape[0]
        locals_.append(
            pltpu.make_async_copy(ref, wo.at[me, pl.ds(at, k), :], local_sem.at[n_in + i])
        )
        at += k
    for copy in locals_:
        copy.start()

    barrier = pltpu.get_barrier_semaphore()
    for d in range(1, n_sp):
        pl.semaphore_signal(barrier, inc=1, device_id=((me + d) % n_sp, t), device_id_type=MESH)
    for d in range(1, n_tp):
        pl.semaphore_signal(barrier, inc=1, device_id=(me, (t + d) % n_tp), device_id_type=MESH)
    pl.semaphore_wait(barrier, n_sp + n_tp - 2)

    sent = []

    def when(cond, fn):
        if cond is None:
            fn()
        else:
            pl.when(cond)(fn)

    def both(a, b):
        return b if a is None else (a if b is None else jnp.logical_and(a, b))

    def send(cond, src, dst, recv, dev):
        copy = pltpu.make_async_remote_copy(
            src_ref=src, dst_ref=dst, send_sem=send_sem.at[len(sent)], recv_sem=recv,
            device_id=dev, device_id_type=MESH,
        )
        when(cond, copy.start)
        sent.append((cond, copy))

    def arrived(cond, dst, recv):
        copy = pltpu.make_async_remote_copy(
            src_ref=dst, dst_ref=dst, send_sem=send_sem.at[0], recv_sem=recv,
            device_id=(me, partner), device_id_type=MESH,
        )
        when(cond, copy.wait_recv)

    up, down = z + 1 < levels, z > 0

    class Spread:
        def __init__(self, buf, main_sem, side_sem):
            self.buf, self.main_sem, self.side_sem = buf, main_sem, side_sem
            k = buf.shape[1]
            self.side = max(16, k // SIDE_SHARE // 16 * 16)
            self.main = k - self.side

        def part(self, s, which):
            if which == "all":
                return self.buf.at[s]
            if which == "main":
                return self.buf.at[s, pl.ds(0, self.main), :]
            return self.buf.at[s, pl.ds(self.main, self.side), :]

        def go(self, cond, s, which, dev_sp):
            sem = self.side_sem if which == "side" else self.main_sem
            ref = self.part(s, which)
            send(cond, ref, ref, sem.at[s], (dev_sp, t))

        def across(self, cond, s, which):
            for d in range(1, cols):
                self.go(cond, s, which, z * cols + (x + d) % cols)

        def peers(self, level):
            return [level * cols + (x + cols - d) % cols for d in range(1, cols)]

        def begin(self):
            self.across(None, me, "side")
            self.go(up, me, "all", me + cols)
            self.go(down, me, "all", me - cols)
            self.across(None, me, "main")

        def begin_side(self):
            for s in self.peers(z):
                arrived(None, self.part(s, "side"), self.side_sem.at[s])
                self.go(up, s, "side", me + cols)
                self.go(down, s, "side", me - cols)

        def hop(self, h):
            for level, there, on, to in (
                (z - h, z - h >= 0, up, me + cols),
                (z + h, z + h < levels, down, me - cols),
            ):
                s = level * cols + x
                arrived(there, self.part(s, "all"), self.main_sem.at[s])
                self.go(both(there, on), s, "all", to)
                self.across(there, s, "main")
                for s in self.peers(level):
                    arrived(there, self.part(s, "side"), self.side_sem.at[s])
                    self.go(both(there, on), s, "side", to)

        def ready(self, h):
            found = []
            for level, there in (
                ((z, None),) if h == 0 else ((z - h, z - h >= 0), (z + h, z + h < levels))
            ):
                found.append((there, level * cols + x, None))
                for s in self.peers(level):
                    found.append(
                        (
                            there,
                            s,
                            functools.partial(
                                arrived, None, self.part(s, "main"), self.main_sem.at[s]
                            ),
                        )
                    )
            return found

    spread_in = Spread(wi, sem_in, sem_in_side)
    spread_out = Spread(wo, sem_out, sem_out_side)
    for copy in locals_[:n_in]:
        copy.wait()
    spread_in.begin()

    mine = pl.ds(pl.multiple_of(t * rows, rows), rows)
    wide = tok[...].astype(F32)
    inverse = lax.rsqrt(jnp.mean(wide * wide, axis=1, keepdims=True) + EPS)
    for i in range(n_sp):
        span = slice(i * piece, (i + 1) * piece)
        xs[i, mine, :] = (tok[:, span].astype(F32) * inverse * gain[:, span]).astype(BF16)

    def rows_of(device):
        return xs.at[:, pl.ds(pl.multiple_of(device * rows, rows), rows), :]

    for d in range(1, chips):
        send(None, rows_of(t), rows_of(t), sem_tok.at[t], (me, (y + d) % chips * CORES + c))
    send(None, rows_of(t), rows_of(t), sem_tok.at[t], (me, partner))

    spread_in.begin_side()
    for h in range(1, levels - 1):
        spread_in.hop(h)
    for copy in locals_[n_in:]:
        copy.wait()

    for d in range(1, chips):
        far = (y + chips - d) % chips * CORES + c
        arrived(None, rows_of(far), sem_tok.at[far])
        send(None, rows_of(far), rows_of(far), sem_tok.at[far], (me, partner))
    arrived(None, rows_of(partner), sem_tok.at[partner])
    for d in range(1, chips):
        far = (y + chips - d) % chips * CORES + (1 - c)
        arrived(None, rows_of(far), sem_tok.at[far])

    tile = row_tile(seq, 256)

    def project(s, first):
        @pl.loop(0, seq // tile)
        def _(i):
            r = pl.ds(pl.multiple_of(i * tile, tile), tile)
            value = jnp.dot(xs[s, r, :], wi[s], preferred_element_type=F32)
            if first:
                acc[r, :] = value
            else:
                acc[r, :] += value

    def project_ready(h):
        for i, (cond, s, wait) in enumerate(spread_in.ready(h)):

            def run(s=s, wait=wait, first=(h == 0 and i == 0)):
                if wait is not None:
                    wait()
                project(s, first)

            when(cond, run)

    for h in range(levels - 1):
        project_ready(h)
    spread_in.hop(levels - 1)
    spread_out.begin()
    project_ready(levels - 1)

    @pl.loop(0, seq // tile)
    def _(i):
        i = seq // tile - 1 - i
        r = pl.multiple_of(i * tile, tile)
        ext[pl.ds(pl.multiple_of(r + WINDOW, WINDOW), tile), :] = acc[pl.ds(r, tile), :].astype(BF16)

    halo = kw + vw + pw
    later, earlier = me + 1 < n_sp, me > 0
    head = ext.at[pl.ds(0, WINDOW), pl.ds(qw, halo)]
    send(later, ext.at[pl.ds(seq, WINDOW), pl.ds(qw, halo)], head, sem_halo.at[0], (me + 1, t))

    channel0 = qw + kw + vw
    group = t * pw // POOL_CH
    whole_prefix = group == POOL_GROUPS - 1
    total = jnp.sum(ext[WINDOW:, channel0:].astype(F32), axis=0, keepdims=True)
    tot[me] = jnp.broadcast_to(total, tot.shape[1:])
    for d in range(1, n_sp):
        send(
            both(whole_prefix, me + d < n_sp), tot.at[me], tot.at[me], sem_tot.at[me],
            (me + d, t),
        )

    group_heads = qw // kw
    stacked = group_heads * WINDOW
    scale = HEAD_DIM ** (-0.5)

    def attend(n):
        q_rows = pl.ds(pl.multiple_of(n * WINDOW + WINDOW, WINDOW), WINDOW)
        k_rows = pl.ds(pl.multiple_of(n * WINDOW, WINDOW), 2 * WINDOW)
        queries = ext[q_rows, :qw]
        keys = ext[k_rows, qw : qw + kw]
        values = ext[k_rows, qw + kw : channel0]
        row = lax.broadcasted_iota(jnp.int32, (stacked, 2 * WINDOW), 0)
        q_index = row % WINDOW
        k_index = lax.broadcasted_iota(jnp.int32, (stacked, 2 * WINDOW), 1)
        lowest = jnp.where(me * blocks + n == 0, WINDOW, 0)
        allowed = (k_index > q_index) & (k_index <= q_index + WINDOW) & (k_index >= lowest)
        which = lax.broadcasted_iota(jnp.int32, (stacked, 1), 0) // WINDOW
        done = []
        for j in range(kw // HEAD_DIM):
            part = slice(j * HEAD_DIM, (j + 1) * HEAD_DIM)
            first = j * group_heads
            q = jnp.concatenate(
                [
                    queries[:, (first + g) * HEAD_DIM : (first + g + 1) * HEAD_DIM]
                    for g in range(group_heads)
                ],
                axis=0,
            )
            scores = (
                lax.dot_general(
                    q, keys[:, part], (((1,), (1,)), ((), ())), preferred_element_type=F32
                )
                * scale
            )
            scores = jnp.where(allowed, scores, -jnp.inf)
            sinks = jnp.full((stacked, 1), sink[first], F32)
            for g in range(1, group_heads):
                sinks = jnp.where(which == g, sink[first + g], sinks)
            peak = jnp.maximum(jnp.max(scores, axis=1, keepdims=True), sinks)
            expo = jnp.exp(scores - peak)
            denom = jnp.sum(expo, axis=1, keepdims=True) + jnp.exp(sinks - peak)
            probs = (expo * (1.0 / denom)).astype(BF16)
            got = jnp.dot(probs, values[:, part], preferred_element_type=F32)
            done += [got[g * WINDOW : (g + 1) * WINDOW] for g in range(group_heads)]
        to = pl.ds(pl.multiple_of(n * WINDOW, WINDOW), WINDOW)
        mix[to, :qw] = jnp.concatenate(done, axis=1).astype(BF16)

    inner = blocks - 1
    stages = max(1, levels - 1)
    cuts = [1 + inner * i // stages for i in range(stages + 1)]
    for i in range(stages):
        pl.loop(cuts[i], cuts[i + 1])(attend)
        if i == 0:
            spread_out.begin_side()
        if i + 1 < levels - 1:
            spread_out.hop(i + 1)

    @pl.when(jnp.logical_not(earlier))
    def _():
        ext[:WINDOW, qw:] = jnp.zeros((WINDOW, halo), BF16)

    arrived(earlier, head, sem_halo.at[0])
    attend(0)

    carry[...] = jnp.zeros(carry.shape, F32)
    for d in range(1, n_sp):

        def add(d=d):
            arrived(None, tot.at[me - d], sem_tot.at[me - d])
            carry[...] += tot[me - d]

        when(both(whole_prefix, me - d >= 0), add)

    reach = jnp.where(
        group == 0, SHORT_REACHES[0], jnp.where(group == 1, SHORT_REACHES[1], WINDOW)
    )
    reach = jnp.where(whole_prefix, n_sp * seq, reach)
    lowest = jnp.where(whole_prefix, WINDOW, 0)

    @pl.loop(0, blocks)
    def _(n):
        q_index = lax.broadcasted_iota(jnp.int32, (WINDOW, 2 * WINDOW), 0)
        k_index = lax.broadcasted_iota(jnp.int32, (WINDOW, 2 * WINDOW), 1)
        distance = q_index + WINDOW - k_index
        band = (distance >= 0) & (distance < reach) & (k_index >= lowest)
        band = jnp.where(band, 1.0, 0.0).astype(BF16)
        k_rows = pl.ds(pl.multiple_of(n * WINDOW, WINDOW), 2 * WINDOW)
        both_blocks = ext[k_rows, channel0:]
        sums = jnp.dot(band, both_blocks, preferred_element_type=F32) + carry[0:1, :]
        position = me * seq + n * WINDOW + lax.broadcasted_iota(jnp.int32, (WINDOW, 1), 0)
        counted = jnp.minimum(position + 1, reach).astype(F32)
        mixed = (sums / counted - both_blocks[WINDOW:].astype(F32)) * pgain[...]
        mix[pl.ds(pl.multiple_of(n * WINDOW, WINDOW), WINDOW), qw:] = mixed.astype(BF16)
        carry[...] = jnp.where(
            whole_prefix, jnp.broadcast_to(sums[WINDOW - 1 :], carry.shape), 0.0
        )

    def mix_rows(chip, core):
        return mix[pl.ds(pl.multiple_of((chip * CORES + core) * rows, rows), rows), :]

    outs = []

    def multiply(cond, s, wait):
        def run():
            if wait is not None:
                wait()
            for chip in range(chips):
                dsend[s, chip] = jnp.dot(
                    mix_rows(chip, 1 - c), wo[s], preferred_element_type=F32
                ).astype(BF16)

        when(cond, run)
        send(cond, dsend.at[s], drecv.at[s], sem_core.at[s], (me, partner))

        def keep():
            for chip in range(chips):
                own[s, chip] = jnp.dot(mix_rows(chip, c), wo[s], preferred_element_type=F32)

        when(cond, keep)

    def finish(cond, s):
        arrived(cond, drecv.at[s], sem_core.at[s])
        for d in range(1, chips):
            far = (y + d) % chips

            def pack(d=d, far=far):
                ysend[s, d - 1] = (own[s, far] + drecv[s, far].astype(F32)).astype(BF16)

            when(cond, pack)
            send(
                cond, ysend.at[s, d - 1], yrecv.at[s, d - 1], sem_y.at[s, d - 1],
                (me, far * CORES + c),
            )

    pending = None
    for h in range(levels):
        if h == levels - 1:
            if pending is not None:
                finish(*pending)
                pending = None
            spread_out.hop(h)
        for cond, s, wait in spread_out.ready(h):
            multiply(cond, s, wait)
            if pending is not None:
                finish(*pending)
            pending = (cond, s)
    finish(*pending)

    for i in range(n_sp):
        value = own[i, y] + drecv[i, y].astype(F32)
        for d in range(1, chips):
            arrived(None, yrecv.at[i, d - 1], sem_y.at[i, d - 1])
            value += yrecv[i, d - 1].astype(F32)
        w = wo.shape[2]
        out[:, i * w : (i + 1) * w] = value.astype(BF16)

    for cond, copy in sent:
        when(cond, copy.wait_send)


def local(
    n_sp, n_tp, tokens_in, norm_gain, query_weight, key_weight, value_weight, pool_weight,
    sink_logit, pool_gain, attention_out_weight, pool_out_weight,
):
    rows, depth = tokens_in.shape
    seq = rows * n_tp
    ins = [query_weight, key_weight, value_weight, pool_weight]
    outs = [attention_out_weight, pool_out_weight]
    widths = tuple(w.shape[1] for w in ins)
    if any(w % 128 for w in widths):
        ins = [jnp.concatenate(ins, axis=1)]
    cols = math.gcd(n_sp, max(1, n_tp // CORES))
    levels, chips = n_sp // cols, n_tp // CORES
    k_in, k_out = ins[0].shape[0], sum(w.shape[0] for w in outs)
    width, out_cols = sum(widths), outs[0].shape[1]
    pw = widths[3]
    hops = 2 * (levels - 1) + 1
    n_send = 2 * (2 + 2 * cols + hops * (2 + 3 * cols)) + 2 * n_tp + n_sp + 2
    n_send += 2 * n_sp * hops * chips
    vmem = pl.BlockSpec(memory_space=pltpu.VMEM)
    hbm = pl.BlockSpec(memory_space=pl.ANY)
    dma = pltpu.SemaphoreType.DMA
    return pl.pallas_call(
        functools.partial(kernel, n_sp, n_tp, cols, len(ins), len(outs), widths),
        out_shape=jax.ShapeDtypeStruct((rows, depth), BF16),
        in_specs=[vmem, vmem, pl.BlockSpec(memory_space=pltpu.SMEM), vmem]
        + [hbm] * (len(ins) + len(outs)),
        out_specs=vmem,
        scratch_shapes=[
            pltpu.VMEM((n_sp, seq, depth // n_sp), BF16),
            pltpu.VMEM((n_sp, k_in, width), BF16),
            pltpu.VMEM((n_sp, k_out, out_cols), BF16),
            pltpu.VMEM((seq, width), F32),
            pltpu.VMEM((seq + WINDOW, width), BF16),
            pltpu.VMEM((seq, widths[0] + pw), BF16),
            pltpu.VMEM((n_sp, 8, pw), F32),
            pltpu.VMEM((8, pw), F32),
            pltpu.VMEM((n_sp, chips, rows, out_cols), BF16),
            pltpu.VMEM((n_sp, chips, rows, out_cols), BF16),
            pltpu.VMEM((n_sp, max(1, chips - 1), rows, out_cols), BF16),
            pltpu.VMEM((n_sp, max(1, chips - 1), rows, out_cols), BF16),
            pltpu.VMEM((n_sp, chips, rows, out_cols), F32),
            dma((len(ins) + len(outs),)),
            dma((n_send,)),
            dma((n_sp,)),
            dma((n_sp,)),
            dma((n_sp,)),
            dma((n_sp,)),
            dma((n_tp,)),
            dma((1,)),
            dma((n_sp,)),
            dma((n_sp,)),
            dma((n_sp, max(1, chips - 1))),
        ],
        compiler_params=pltpu.CompilerParams(
            collective_id=0, has_side_effects=True, vmem_limit_bytes=58 << 20
        ),
    )(
        tokens_in, norm_gain.reshape(1, -1), sink_logit, pool_gain.reshape(1, -1), *ins, *outs
    )


def solution(mesh):
    in_specs = (
        P(("sp", "tp"), None), P(), P("sp", "tp"), P("sp", "tp"), P("sp", "tp"), P("sp", "tp"),
        P("tp"), P("tp"), P("tp", "sp"), P("tp", "sp"),
    )
    out_specs = P(("sp", "tp"), None)
    return jax.shard_map(
        functools.partial(local, mesh.shape["sp"], mesh.shape["tp"]),
        mesh=mesh, in_specs=in_specs, out_specs=out_specs, check_vma=False,
    )
```

time: 259 us -> 92.8 us (0.36)
  waiting for transfers between devices: 117 us -> 0 us
  Pallas kernels: 0 us -> 90.6 us
  blocking collectives: 84 us -> 0 us
  matrix products: 22.9 us -> 0 us
  between operations: 13.8 us -> 0.01 us
  starting transfers between devices: 8.61 us -> 0 us
  other arithmetic: 6.68 us -> 0 us
  local copies, waits for them, and re-layouts: 5.6 us -> 2.09 us
    pallas_call x0 -> x1, Pallas kernels: none -> 90.6 us  [local(): pl.pallas_call(functools.partial(kernel, n_sp, n_tp, cols, len(ins), len(...]
    all_gather x3 -> x0, blocking collectives: 84 us -> none  [the longest x1 33.1 us: local(): lax.all_gather(key_weight, 'sp', axis=0, tiled=True)]
    all_gather x5 -> x0, waiting for transfers between devices: 77.3 us -> none  [the longest x1 35.4 us: local(): lax.all_gather(query_weight, 'sp', axis=0, tiled=True)]
    reduce_scatter x1 -> x0, waiting for transfers between devices: 37 us -> none  [local(): lax.psum_scatter((jnp.dot(attended, out_attend, preferred_element_type=jn...]
    dot_general x8 -> x0, matrix products: 22.9 us -> none  [the longest x4 10.3 us: local(): jnp.dot(all_rows, weight_piece, preferred_element_type=jnp.float32)]
    ppermute x3 -> x0, starting transfers between devices: 8.42 us -> none  [passed_along(): return lax.ppermute(block, axis, route)]
    slice x12 -> x0, local copies, waits for them, and re-layouts: 4.59 us -> none  [the longest x4 1.68 us: local(): key_pairs = jnp.concatenate([key_ext[:-1], key_ext[1:]], axis=1)]
  transfers between devices with their start and end apart: 9 -> 0, of which waited for: 5 -> 0; matrix products, arithmetic and copies ran while one was open for 10% -> 0% of each run, Pallas kernels for 0% -> 0%
where the time goes in v1:
time: 92.8 us; the launch traced here: 92.6 us
  Pallas kernels  90.6 us (98%)
  local copies, waits for them, and re-layouts  2.09 us (2%)
    pallas_call x1, Pallas kernels, local(): pl.pallas_call(functools.partial(kernel, n_sp, n_tp, cols, len(ins), len(...  90.6 us
    unnamed x1, local copies, waits for them, and re-layouts  2.09 us

profile of v1, /device:TPU:0, one launch (start us, length us, event | category | flops | bytes accessed | tf_op | source)
XLA Modules:
  0.0 92.6 jit_solution(1627503490997756473)
XLA Ops:
  0.0 90.6 %shard_map.100 = bf16[192,2048]{1,0:T(8,128)(2,1)} custom-call(bf16[192,2048]{1,0:T(8,128)(2,1)} %refs_0_.1, f32[1,2048]{1,0:T(1,128)} %bitcast.2, f32[4]{0:T(128)} %refs_2_.1, f32[1,256]{1,0:T(1,128)} %bitcast.3, bf16[256,256]{1,0:T(8,128)(2,1)} %refs_4_.1, bf16[256,128]{1,0:T(8,128)(2,1)} %refs_5_.1, bf16[256,128]{1,0:T(8,128)(2,1)} %refs_6_.1, ...), custom_call_target="tpu_custom_call" | custom-call | tf_op jit(solution)/shard_map/pallas_call | solution.py:437
  90.6 2.1 %copy.12 = bf16[192,2048]{1,0:T(8,128)(2,1)} copy(bf16[192,2048]{1,0:T(8,128)(2,1)} %shard_map.100) | data formatting | bytes 1572864

commit v2 on v1

--- a/solution.py
+++ b/solution.py
@@ -15,7 +15,7 @@
 EPS = 1e-06
 SHORT_REACHES = (8, 32)
 CORES = 2
-SIDE_SHARE = 6
+SIDE_SHARE = 0.4
 MESH = pl.DeviceIdType.MESH
 F32 = jnp.float32
 BF16 = jnp.bfloat16
@@ -33,14 +33,15 @@
     win_refs = refs[4 : 4 + n_in]
     wout_refs = refs[4 + n_in : 4 + n_in + n_out]
     (
-        out, xs, wi, wo, acc, ext, mix, tot, carry, dsend, drecv, ysend, yrecv, own,
-        local_sem, send_sem, sem_in, sem_in_side, sem_out, sem_out_side,
+        out, tokv, xs, wq, wp, wo, accq, accp, ext, mix, tot, carry, dsend, drecv, ysend, yrecv, own,
+        local_sem, send_sem, sem_q, sem_p, sem_out, sem_out_side,
         sem_tok, sem_halo, sem_tot, sem_core, sem_y,
     ) = refs[4 + n_in + n_out :]
     qw, kw, vw, pw = widths
     levels = n_sp // cols
     chips = n_tp // CORES
     rows, seq = tok.shape[0], xs.shape[1]
+    qkv = wq.shape[2]
     piece = xs.shape[2]
     blocks = seq // WINDOW
     me, t = lax.axis_index("sp"), lax.axis_index("tp")
@@ -50,10 +51,11 @@
 
     locals_ = []
     at = 0
-    for i, ref in enumerate(win_refs):
+    for i, ref in enumerate(win_refs[:-1]):
         w = ref.shape[1]
-        locals_.append(pltpu.make_async_copy(ref, wi.at[me, :, pl.ds(at, w)], local_sem.at[i]))
+        locals_.append(pltpu.make_async_copy(ref, wq.at[me, :, pl.ds(at, w)], local_sem.at[i]))
         at += w
+    locals_.append(pltpu.make_async_copy(win_refs[-1], wp.at[me], local_sem.at[n_in - 1]))
     at = 0
     for i, ref in enumerate(wout_refs):
         k = ref.shape[0]
@@ -61,7 +63,8 @@
             pltpu.make_async_copy(ref, wo.at[me, pl.ds(at, k), :], local_sem.at[n_in + i])
         )
         at += k
-    for copy in locals_:
+    tok_copy = pltpu.make_async_copy(tok, tokv, local_sem.at[n_in + n_out])
+    for copy in locals_[:n_in] + [tok_copy] + locals_[n_in:]:
         copy.start()
 
     barrier = pltpu.get_barrier_semaphore()
@@ -103,7 +106,7 @@
         def __init__(self, buf, main_sem, side_sem):
             self.buf, self.main_sem, self.side_sem = buf, main_sem, side_sem
             k = buf.shape[1]
-            self.side = max(16, k // SIDE_SHARE // 16 * 16)
+            self.side = 0 if side_sem is None else max(16, int(k * SIDE_SHARE) // 16 * 16)
             self.main = k - self.side
 
         def part(self, s, which):
@@ -114,6 +117,8 @@
             return self.buf.at[s, pl.ds(self.main, self.side), :]
 
         def go(self, cond, s, which, dev_sp):
+            if which == "side" and not self.side:
+                return
             sem = self.side_sem if which == "side" else self.main_sem
             ref = self.part(s, which)
             send(cond, ref, ref, sem.at[s], (dev_sp, t))
@@ -132,7 +137,7 @@
             self.across(None, me, "main")
 
         def begin_side(self):
-            for s in self.peers(z):
+            for s in self.peers(z) if self.side else []:
                 arrived(None, self.part(s, "side"), self.side_sem.at[s])
                 self.go(up, s, "side", me + cols)
                 self.go(down, s, "side", me - cols)
@@ -146,7 +151,7 @@
                 arrived(there, self.part(s, "all"), self.main_sem.at[s])
                 self.go(both(there, on), s, "all", to)
                 self.across(there, s, "main")
-                for s in self.peers(level):
+                for s in self.peers(level) if self.side else []:
                     arrived(there, self.part(s, "side"), self.side_sem.at[s])
                     self.go(both(there, on), s, "side", to)
 
@@ -168,18 +173,21 @@
                     )
             return found
 
-    spread_in = Spread(wi, sem_in, sem_in_side)
+    spread_q = Spread(wq, sem_q, None)
+    spread_p = Spread(wp, sem_p, None)
     spread_out = Spread(wo, sem_out, sem_out_side)
     for copy in locals_[:n_in]:
         copy.wait()
-    spread_in.begin()
+    spread_q.begin()
+    spread_p.begin()
+    tok_copy.wait()
 
     mine = pl.ds(pl.multiple_of(t * rows, rows), rows)
-    wide = tok[...].astype(F32)
+    wide = tokv[...].astype(F32)
     inverse = lax.rsqrt(jnp.mean(wide * wide, axis=1, keepdims=True) + EPS)
     for i in range(n_sp):
         span = slice(i * piece, (i + 1) * piece)
-        xs[i, mine, :] = (tok[:, span].astype(F32) * inverse * gain[:, span]).astype(BF16)
+        xs[i, mine, :] = (tokv[:, span].astype(F32) * inverse * gain[:, span]).astype(BF16)
 
     def rows_of(device):
         return xs.at[:, pl.ds(pl.multiple_of(device * rows, rows), rows), :]
@@ -188,11 +196,10 @@
         send(None, rows_of(t), rows_of(t), sem_tok.at[t], (me, (y + d) % chips * CORES + c))
     send(None, rows_of(t), rows_of(t), sem_tok.at[t], (me, partner))
 
-    spread_in.begin_side()
     for h in range(1, levels - 1):
-        spread_in.hop(h)
-    for copy in locals_[n_in:]:
-        copy.wait()
+        spread_q.hop(h)
+        if h < levels - 2:
+            spread_p.hop(h)
 
     for d in range(1, chips):
         far = (y + chips - d) % chips * CORES + c
@@ -203,55 +210,57 @@
         far = (y + chips - d) % chips * CORES + (1 - c)
         arrived(None, rows_of(far), sem_tok.at[far])
 
+    spread_q.hop(levels - 1)
+    for h in range(max(1, levels - 2), levels - 1):
+        spread_p.hop(h)
+
     tile = row_tile(seq, 256)
 
-    def project(s, first):
-        @pl.loop(0, seq // tile)
-        def _(i):
-            r = pl.ds(pl.multiple_of(i * tile, tile), tile)
-            value = jnp.dot(xs[s, r, :], wi[s], preferred_element_type=F32)
-            if first:
-                acc[r, :] = value
-            else:
-                acc[r, :] += value
-
-    def project_ready(h):
-        for i, (cond, s, wait) in enumerate(spread_in.ready(h)):
+    def project(spread, acc, h):
+        for i, (cond, s, wait) in enumerate(spread.ready(h)):
 
             def run(s=s, wait=wait, first=(h == 0 and i == 0)):
                 if wait is not None:
                     wait()
-                project(s, first)
+
+                @pl.loop(0, seq // tile)
+                def _(i):
+                    r = pl.ds(pl.multiple_of(i * tile, tile), tile)
+                    value = jnp.dot(xs[s, r, :], spread.buf[s], preferred_element_type=F32)
+                    if first:
+                        acc[r, :] = value
+                    else:
+                        acc[r, :] += value
 
             when(cond, run)
 
+    def settle(acc, at):
+        @pl.loop(0, seq // tile)
+        def _(i):
+            r = pl.multiple_of(i * tile, tile)
+            to = pl.ds(pl.multiple_of(r + WINDOW, WINDOW), tile)
+            ext[to, at : at + acc.shape[1]] = acc[pl.ds(r, tile), :].astype(BF16)
+
+    later, earlier = me + 1 < n_sp, me > 0
+
+    def pass_on(at, width, i):
+        head = ext.at[pl.ds(0, WINDOW), pl.ds(at, width)]
+        tail = ext.at[pl.ds(seq, WINDOW), pl.ds(at, width)]
+        send(later, tail, head, sem_halo.at[i], (me + 1, t))
+        return head
+
     for h in range(levels - 1):
-        project_ready(h)
-    spread_in.hop(levels - 1)
+        project(spread_q, accq, h)
+    spread_p.hop(levels - 1)
+    for copy in locals_[n_in:]:
+        copy.wait()
     spread_out.begin()
-    project_ready(levels - 1)
-
-    @pl.loop(0, seq // tile)
-    def _(i):
-        i = seq // tile - 1 - i
-        r = pl.multiple_of(i * tile, tile)
-        ext[pl.ds(pl.multiple_of(r + WINDOW, WINDOW), tile), :] = acc[pl.ds(r, tile), :].astype(BF16)
-
-    halo = kw + vw + pw
-    later, earlier = me + 1 < n_sp, me > 0
-    head = ext.at[pl.ds(0, WINDOW), pl.ds(qw, halo)]
-    send(later, ext.at[pl.ds(seq, WINDOW), pl.ds(qw, halo)], head, sem_halo.at[0], (me + 1, t))
-
-    channel0 = qw + kw + vw
+    project(spread_q, accq, levels - 1)
+    settle(accq, 0)
+    head_kv = pass_on(qw, kw + vw, 0)
+    channel0 = qkv
     group = t * pw // POOL_CH
     whole_prefix = group == POOL_GROUPS - 1
-    total = jnp.sum(ext[WINDOW:, channel0:].astype(F32), axis=0, keepdims=True)
-    tot[me] = jnp.broadcast_to(total, tot.shape[1:])
-    for d in range(1, n_sp):
-        send(
-            both(whole_prefix, me + d < n_sp), tot.at[me], tot.at[me], sem_tot.at[me],
-            (me + d, t),
-        )
 
     group_heads = qw // kw
     stacked = group_heads * WINDOW
@@ -299,22 +308,31 @@
         to = pl.ds(pl.multiple_of(n * WINDOW, WINDOW), WINDOW)
         mix[to, :qw] = jnp.concatenate(done, axis=1).astype(BF16)
 
-    inner = blocks - 1
-    stages = max(1, levels - 1)
-    cuts = [1 + inner * i // stages for i in range(stages + 1)]
-    for i in range(stages):
-        pl.loop(cuts[i], cuts[i + 1])(attend)
-        if i == 0:
-            spread_out.begin_side()
-        if i + 1 < levels - 1:
-            spread_out.hop(i + 1)
+    spread_out.begin_side()
+    spread_out.hop(1)
+    third = max(2, (blocks + 1) // 2)
+    pl.loop(1, third)(attend)
+    spread_out.hop(2)
+    for h in range(levels):
+        project(spread_p, accp, h)
+    settle(accp, channel0)
+    head_pool = pass_on(channel0, pw, 1)
+    total = jnp.sum(ext[WINDOW:, channel0:].astype(F32), axis=0, keepdims=True)
+    tot[me] = jnp.broadcast_to(total, tot.shape[1:])
+    for d in range(1, n_sp):
+        send(
+            both(whole_prefix, me + d < n_sp), tot.at[me], tot.at[me], sem_tot.at[me],
+            (me + d, t),
+        )
+    pl.loop(third, blocks)(attend)
 
     @pl.when(jnp.logical_not(earlier))
     def _():
-        ext[:WINDOW, qw:] = jnp.zeros((WINDOW, halo), BF16)
-
-    arrived(earlier, head, sem_halo.at[0])
+        ext[:WINDOW, qw:] = jnp.zeros((WINDOW, ext.shape[1] - qw), BF16)
+
+    arrived(earlier, head_kv, sem_halo.at[0])
     attend(0)
+    arrived(earlier, head_pool, sem_halo.at[1])
 
     carry[...] = jnp.zeros(carry.shape, F32)
     for d in range(1, n_sp):
@@ -422,14 +440,14 @@
     outs = [attention_out_weight, pool_out_weight]
     widths = tuple(w.shape[1] for w in ins)
     if any(w % 128 for w in widths):
-        ins = [jnp.concatenate(ins, axis=1)]
+        ins = [jnp.concatenate(ins[:3], axis=1), ins[3]]
     cols = math.gcd(n_sp, max(1, n_tp // CORES))
     levels, chips = n_sp // cols, n_tp // CORES
     k_in, k_out = ins[0].shape[0], sum(w.shape[0] for w in outs)
     width, out_cols = sum(widths), outs[0].shape[1]
     pw = widths[3]
     hops = 2 * (levels - 1) + 1
-    n_send = 2 * (2 + 2 * cols + hops * (2 + 3 * cols)) + 2 * n_tp + n_sp + 2
+    n_send = 3 * (2 + 2 * cols + hops * (2 + 3 * cols)) + 2 * n_tp + n_sp + 2
     n_send += 2 * n_sp * hops * chips
     vmem = pl.BlockSpec(memory_space=pltpu.VMEM)
     hbm = pl.BlockSpec(memory_space=pl.ANY)
@@ -437,14 +455,17 @@
     return pl.pallas_call(
         functools.partial(kernel, n_sp, n_tp, cols, len(ins), len(outs), widths),
         out_shape=jax.ShapeDtypeStruct((rows, depth), BF16),
-        in_specs=[vmem, vmem, pl.BlockSpec(memory_space=pltpu.SMEM), vmem]
+        in_specs=[hbm, vmem, pl.BlockSpec(memory_space=pltpu.SMEM), vmem]
         + [hbm] * (len(ins) + len(outs)),
         out_specs=vmem,
         scratch_shapes=[
+            pltpu.VMEM((rows, depth), BF16),
             pltpu.VMEM((n_sp, seq, depth // n_sp), BF16),
-            pltpu.VMEM((n_sp, k_in, width), BF16),
+            pltpu.VMEM((n_sp, k_in, width - pw), BF16),
+            pltpu.VMEM((n_sp, k_in, pw), BF16),
             pltpu.VMEM((n_sp, k_out, out_cols), BF16),
-            pltpu.VMEM((seq, width), F32),
+            pltpu.VMEM((seq, width - pw), F32),
+            pltpu.VMEM((seq, pw), F32),
             pltpu.VMEM((seq + WINDOW, width), BF16),
             pltpu.VMEM((seq, widths[0] + pw), BF16),
             pltpu.VMEM((n_sp, 8, pw), F32),
@@ -454,14 +475,14 @@
             pltpu.VMEM((n_sp, max(1, chips - 1), rows, out_cols), BF16),
             pltpu.VMEM((n_sp, max(1, chips - 1), rows, out_cols), BF16),
             pltpu.VMEM((n_sp, chips, rows, out_cols), F32),
-            dma((len(ins) + len(outs),)),
+            dma((len(ins) + len(outs) + 1,)),
             dma((n_send,)),
             dma((n_sp,)),
             dma((n_sp,)),
             dma((n_sp,)),
             dma((n_sp,)),
             dma((n_tp,)),
-            dma((1,)),
+            dma((2,)),
             dma((n_sp,)),
             dma((n_sp,)),
             dma((n_sp, max(1, chips - 1))),

time: 92.8 us -> 97.9 us (1.055)
  Pallas kernels: 90.6 us -> 95.2 us
    pallas_call x1, Pallas kernels: 90.6 us -> 95.2 us  [local(): pl.pallas_call(functools.partial(kernel, n_sp, n_tp, cols, len(ins), len(...]
where the time goes in v2:
time: 97.9 us; the launch traced here: 97.3 us
  Pallas kernels  95.2 us (97%)
  local copies, waits for them, and re-layouts  2.09 us (2%)
    pallas_call x1, Pallas kernels, local(): pl.pallas_call(functools.partial(kernel, n_sp, n_tp, cols, len(ins), len(...  95.2 us
    unnamed x1, local copies, waits for them, and re-layouts  2.09 us

profile of v2, /device:TPU:0, one launch (start us, length us, event | category | flops | bytes accessed | tf_op | source)
XLA Modules:
  0.0 97.3 jit_solution(7476241231044553350)
XLA Ops:
  0.0 95.2 %shard_map.100 = bf16[192,2048]{1,0:T(8,128)(2,1)} custom-call(bf16[192,2048]{1,0:T(8,128)(2,1)} %refs_0_.1, f32[1,2048]{1,0:T(1,128)} %bitcast.2, f32[4]{0:T(128)} %refs_2_.1, f32[1,256]{1,0:T(1,128)} %bitcast.3, bf16[256,256]{1,0:T(8,128)(2,1)} %refs_4_.1, bf16[256,128]{1,0:T(8,128)(2,1)} %refs_5_.1, bf16[256,128]{1,0:T(8,128)(2,1)} %refs_6_.1, ...), custom_call_target="tpu_custom_call" | custom-call | tf_op jit(solution)/shard_map/pallas_call | solution.py:455
  95.2 2.1 %copy.12 = bf16[192,2048]{1,0:T(8,128)(2,1)} copy(bf16[192,2048]{1,0:T(8,128)(2,1)} %shard_map.100) | data formatting | bytes 1572864

commit v3 on v2

--- a/solution.py
+++ b/solution.py
@@ -15,7 +15,7 @@
 EPS = 1e-06
 SHORT_REACHES = (8, 32)
 CORES = 2
-SIDE_SHARE = 0.4
+SIDE_SHARE = 0.3
 MESH = pl.DeviceIdType.MESH
 F32 = jnp.float32
 BF16 = jnp.bfloat16
@@ -34,7 +34,7 @@
     wout_refs = refs[4 + n_in : 4 + n_in + n_out]
     (
         out, tokv, xs, wq, wp, wo, accq, accp, ext, mix, tot, carry, dsend, drecv, ysend, yrecv, own,
-        local_sem, send_sem, sem_q, sem_p, sem_out, sem_out_side,
+        local_sem, send_sem, sem_q, sem_p, sem_p_side, sem_out, sem_out_side,
         sem_tok, sem_halo, sem_tot, sem_core, sem_y,
     ) = refs[4 + n_in + n_out :]
     qw, kw, vw, pw = widths
@@ -174,7 +174,7 @@
             return found
 
     spread_q = Spread(wq, sem_q, None)
-    spread_p = Spread(wp, sem_p, None)
+    spread_p = Spread(wp, sem_p, sem_p_side)
     spread_out = Spread(wo, sem_out, sem_out_side)
     for copy in locals_[:n_in]:
         copy.wait()
@@ -198,8 +198,9 @@
 
     for h in range(1, levels - 1):
         spread_q.hop(h)
-        if h < levels - 2:
-            spread_p.hop(h)
+    spread_p.begin_side()
+    for h in range(1, levels - 2):
+        spread_p.hop(h)
 
     for d in range(1, chips):
         far = (y + chips - d) % chips * CORES + c
@@ -213,6 +214,9 @@
     spread_q.hop(levels - 1)
     for h in range(max(1, levels - 2), levels - 1):
         spread_p.hop(h)
+    for copy in locals_[n_in:]:
+        copy.wait()
+    spread_out.begin()
 
     tile = row_tile(seq, 256)
 
@@ -252,9 +256,6 @@
     for h in range(levels - 1):
         project(spread_q, accq, h)
     spread_p.hop(levels - 1)
-    for copy in locals_[n_in:]:
-        copy.wait()
-    spread_out.begin()
     project(spread_q, accq, levels - 1)
     settle(accq, 0)
     head_kv = pass_on(qw, kw + vw, 0)
@@ -312,7 +313,6 @@
     spread_out.hop(1)
     third = max(2, (blocks + 1) // 2)
     pl.loop(1, third)(attend)
-    spread_out.hop(2)
     for h in range(levels):
         project(spread_p, accp, h)
     settle(accp, channel0)
@@ -332,6 +332,8 @@
 
     arrived(earlier, head_kv, sem_halo.at[0])
     attend(0)
+    for h in range(2, levels - 1):
+        spread_out.hop(h)
     arrived(earlier, head_pool, sem_halo.at[1])
 
     carry[...] = jnp.zeros(carry.shape, F32)
@@ -399,11 +401,13 @@
                 ysend[s, d - 1] = (own[s, far] + drecv[s, far].astype(F32)).astype(BF16)
 
             when(cond, pack)
+            last.append(len(sent))
             send(
                 cond, ysend.at[s, d - 1], yrecv.at[s, d - 1], sem_y.at[s, d - 1],
                 (me, far * CORES + c),
             )
 
+    last = []
     pending = None
     for h in range(levels):
         if h == levels - 1:
@@ -418,6 +422,10 @@
             pending = (cond, s)
     finish(*pending)
 
+    for i, (cond, copy) in enumerate(sent):
+        if i not in last:
+            when(cond, copy.wait_send)
+
     for i in range(n_sp):
         value = own[i, y] + drecv[i, y].astype(F32)
         for d in range(1, chips):
@@ -426,8 +434,8 @@
         w = wo.shape[2]
         out[:, i * w : (i + 1) * w] = value.astype(BF16)
 
-    for cond, copy in sent:
-        when(cond, copy.wait_send)
+    for i in last:
+        when(sent[i][0], sent[i][1].wait_send)
 
 
 def local(
@@ -481,6 +489,7 @@
             dma((n_sp,)),
             dma((n_sp,)),
             dma((n_sp,)),
+            dma((n_sp,)),
             dma((n_tp,)),
             dma((2,)),
             dma((n_sp,)),

time: 97.9 us -> 85.8 us (0.88)
  Pallas kernels: 95.2 us -> 83.5 us
    pallas_call x1, Pallas kernels: 95.2 us -> 83.5 us  [local(): pl.pallas_call(functools.partial(kernel, n_sp, n_tp, cols, len(ins), len(...]
where the time goes in v3:
time: 85.8 us; the launch traced here: 85.6 us
  Pallas kernels  83.5 us (97%)
  local copies, waits for them, and re-layouts  2.09 us (2%)
    pallas_call x1, Pallas kernels, local(): pl.pallas_call(functools.partial(kernel, n_sp, n_tp, cols, len(ins), len(...  83.5 us
    unnamed x1, local copies, waits for them, and re-layouts  2.09 us

profile of v3, /device:TPU:0, one launch (start us, length us, event | category | flops | bytes accessed | tf_op | source)
XLA Modules:
  0.0 85.6 jit_solution(10450331292942494342)
XLA Ops:
  0.0 83.5 %shard_map.100 = bf16[192,2048]{1,0:T(8,128)(2,1)} custom-call(bf16[192,2048]{1,0:T(8,128)(2,1)} %refs_0_.1, f32[1,2048]{1,0:T(1,128)} %bitcast.2, f32[4]{0:T(128)} %refs_2_.1, f32[1,256]{1,0:T(1,128)} %bitcast.3, bf16[256,256]{1,0:T(8,128)(2,1)} %refs_4_.1, bf16[256,128]{1,0:T(8,128)(2,1)} %refs_5_.1, bf16[256,128]{1,0:T(8,128)(2,1)} %refs_6_.1, ...), custom_call_target="tpu_custom_call" | custom-call | tf_op jit(solution)/shard_map/pallas_call | solution.py:463
  83.5 2.1 %copy.12 = bf16[192,2048]{1,0:T(8,128)(2,1)} copy(bf16[192,2048]{1,0:T(8,128)(2,1)} %shard_map.100) | data formatting | bytes 1572864

commit v4 on v3

--- a/solution.py
+++ b/solution.py
@@ -142,18 +142,28 @@
                 self.go(up, s, "side", me + cols)
                 self.go(down, s, "side", me - cols)
 
-        def hop(self, h):
-            for level, there, on, to in (
+        def ways(self, h):
+            return (
                 (z - h, z - h >= 0, up, me + cols),
                 (z + h, z + h < levels, down, me - cols),
-            ):
+            )
+
+        def hop_main(self, h):
+            for level, there, on, to in self.ways(h):
                 s = level * cols + x
                 arrived(there, self.part(s, "all"), self.main_sem.at[s])
                 self.go(both(there, on), s, "all", to)
                 self.across(there, s, "main")
-                for s in self.peers(level) if self.side else []:
+
+        def hop_side(self, h):
+            for level, there, on, to in self.ways(h) if self.side else ():
+                for s in self.peers(level):
                     arrived(there, self.part(s, "side"), self.side_sem.at[s])
                     self.go(both(there, on), s, "side", to)
+
+        def hop(self, h):
+            self.hop_main(h)
+            self.hop_side(h)
 
         def ready(self, h):
             found = []
@@ -309,10 +319,10 @@
         to = pl.ds(pl.multiple_of(n * WINDOW, WINDOW), WINDOW)
         mix[to, :qw] = jnp.concatenate(done, axis=1).astype(BF16)
 
-    spread_out.begin_side()
-    spread_out.hop(1)
     third = max(2, (blocks + 1) // 2)
     pl.loop(1, third)(attend)
+    spread_out.hop_main(1)
+    pl.loop(third, blocks)(attend)
     for h in range(levels):
         project(spread_p, accp, h)
     settle(accp, channel0)
@@ -324,7 +334,10 @@
             both(whole_prefix, me + d < n_sp), tot.at[me], tot.at[me], sem_tot.at[me],
             (me + d, t),
         )
-    pl.loop(third, blocks)(attend)
+    for h in range(2, levels - 1):
+        spread_out.hop_main(h)
+    spread_out.begin_side()
+    spread_out.hop_side(1)
 
     @pl.when(jnp.logical_not(earlier))
     def _():
@@ -333,7 +346,7 @@
     arrived(earlier, head_kv, sem_halo.at[0])
     attend(0)
     for h in range(2, levels - 1):
-        spread_out.hop(h)
+        spread_out.hop_side(h)
     arrived(earlier, head_pool, sem_halo.at[1])
 
     carry[...] = jnp.zeros(carry.shape, F32)

time: 85.8 us -> 87.7 us (1.022)
  Pallas kernels: 83.5 us -> 85.4 us
    pallas_call x1, Pallas kernels: 83.5 us -> 85.4 us  [local(): pl.pallas_call(functools.partial(kernel, n_sp, n_tp, cols, len(ins), len(...]
where the time goes in v4:
time: 87.7 us; the launch traced here: 87.5 us
  Pallas kernels  85.4 us (97%)
  local copies, waits for them, and re-layouts  2.09 us (2%)
    pallas_call x1, Pallas kernels, local(): pl.pallas_call(functools.partial(kernel, n_sp, n_tp, cols, len(ins), len(...  85.4 us
    unnamed x1, local copies, waits for them, and re-layouts  2.09 us

profile of v4, /device:TPU:0, one launch (start us, length us, event | category | flops | bytes accessed | tf_op | source)
XLA Modules:
  0.0 87.5 jit_solution(9490277943070673736)
XLA Ops:
  0.0 85.4 %shard_map.100 = bf16[192,2048]{1,0:T(8,128)(2,1)} custom-call(bf16[192,2048]{1,0:T(8,128)(2,1)} %refs_0_.1, f32[1,2048]{1,0:T(1,128)} %bitcast.2, f32[4]{0:T(128)} %refs_2_.1, f32[1,256]{1,0:T(1,128)} %bitcast.3, bf16[256,256]{1,0:T(8,128)(2,1)} %refs_4_.1, bf16[256,128]{1,0:T(8,128)(2,1)} %refs_5_.1, bf16[256,128]{1,0:T(8,128)(2,1)} %refs_6_.1, ...), custom_call_target="tpu_custom_call" | custom-call | tf_op jit(solution)/shard_map/pallas_call | solution.py:476
  85.4 2.1 %copy.12 = bf16[192,2048]{1,0:T(8,128)(2,1)} copy(bf16[192,2048]{1,0:T(8,128)(2,1)} %shard_map.100) | data formatting | bytes 1572864
